TPU v7x, 32 devices: a whole 2x2x4 slice. The times are simulated.
32 devices in a mesh: ep: 32 (over z, y, x, core).
Axes of the slice: x: 2, y: 2, z: 4, core: 2. Of those that a mesh axis runs over, the one named last changes fastest.
Arguments:
- hidden_in: bfloat16 [64, 2048], P('ep'), may hold values from -6 to 6
- lengths: int32 [64], P('ep'), may hold values from 1 to 1024, as said below
- key_cache: bfloat16 [64, 1024, 512], P('ep'), may hold values from -30 to 30
- value_cache: bfloat16 [64, 1024, 512], P('ep'), may hold values from -6 to 6
- query_w: bfloat16 [2048, 2048], P('ep'), may hold values from -0.125 to 0.125
- key_w: bfloat16 [2048, 512], P('ep'), may hold values from -0.125 to 0.125
- value_w: bfloat16 [2048, 512], P('ep'), may hold values from -0.125 to 0.125
- out_w: bfloat16 [2048, 2048], P('ep'), may hold values from -0.125 to 0.125
- lam_heads: float32 [8], replicated, may hold values from 0.3 to 0.8
- head_gain: float32 [256], replicated, may hold values from 0.1 to 1.9
- attn_gain: float32 [2048], replicated, may hold values from 0.1 to 1.9
- moe_gain: float32 [2048], replicated, may hold values from 0.1 to 1.9
- routing: int32 [64, 6], replicated, may hold values from 0 to 31, all different within a row; in each aligned block of 64 rows (0 to 63, 64 to 127, ...) at most 24 rows name the same one
- route_weight: float32 [64, 6], replicated, may hold values from 0.1 to 0.6
- gate_w: bfloat16 [32, 2048, 512], P('ep'), may hold values from -0.125 to 0.125
- up_w: bfloat16 [32, 2048, 512], P('ep'), may hold values from -0.125 to 0.125
- down_w: bfloat16 [32, 512, 2048], P('ep'), may hold values from -0.25 to 0.25
- shared_gate: bfloat16 [2048, 512], replicated, may hold values from -0.125 to 0.125
- shared_up: bfloat16 [2048, 512], replicated, may hold values from -0.125 to 0.125
- shared_down: bfloat16 [512, 2048], replicated, may hold values from -0.25 to 0.25
Outputs:
- layer_out: bfloat16 [64, 2048], P('ep')
- key_new: bfloat16 [64, 512], P('ep')
- value_new: bfloat16 [64, 512], P('ep')
Inputs may be any that keep to these rules, and one draw needn't show every extreme that they name: `lengths`: some sequence has exactly 1024 positions in use. `routing`: each row names 6 different experts; no expert is named by more than 24 rows, a bound that some block reaches.
All inputs are finite; a program needn't handle non-finite values.
Results may differ from a plain program's by a relative error of at most 0.013.
The roundings to bfloat16 on the way count: a program that leaves them out, or rounds other values in their place, can miss the bound.
Values may be sent and summed in bfloat16 or wider, within the bound.
A program may use at most 64 MiB of HBM per device.

v0:
```python
import jax
import jax.numpy as jnp
from jax import lax
from jax.sharding import PartitionSpec as P

KV_HEADS = 2
HEAD_DIM = 128
EXP_CAP = 24
eps_norm = 1e-06
eps_head = 1e-05
theta_base = 500000.0


def rms_scale(row_block, gain_vec, epsilon):
    row_block = row_block.astype(jnp.float32)
    return (
        row_block
        * lax.rsqrt(jnp.mean(row_block * row_block, axis=-1, keepdims=True) + epsilon)
        * gain_vec
    )


def rotate(vectors, positions):
    half_width = vectors.shape[-1] // 2
    inverse = theta_base ** (-jnp.arange(half_width, dtype=jnp.float32) / half_width)
    angles = positions.astype(jnp.float32)[..., None] * inverse
    cosine, sine_part = (jnp.cos(angles), jnp.sin(angles))
    lower_half, upper_half = (vectors[..., :half_width], vectors[..., half_width:])
    return jnp.concatenate(
        [
            lower_half * cosine - upper_half * sine_part,
            lower_half * sine_part + upper_half * cosine,
        ],
        axis=-1,
    )


def attend(queries, key_new, value_new, cache_keys, cache_values, lengths, lam_heads, head_gain):
    num_seqs, kv_heads, group_size = (queries.shape[0], queries.shape[1], queries.shape[2])
    head_dim = queries.shape[-1]
    cache_len = cache_keys.shape[1]
    cache_keys = cache_keys.reshape(num_seqs, cache_len, kv_heads, 2, head_dim)
    cache_values = cache_values.reshape(num_seqs, cache_len, kv_heads, -1)
    value_new = value_new.reshape(num_seqs, kv_heads, -1)
    score_scale = head_dim ** (-0.5)
    scores = (
        jnp.einsum("skgph,sckph->skgpc", queries, cache_keys, preferred_element_type=jnp.float32)
        * score_scale
    )
    self_score = (
        jnp.einsum("skgph,skph->skgp", queries, key_new, preferred_element_type=jnp.float32)
        * score_scale
    )
    live_mask = (jnp.arange(cache_len)[None, :] < lengths[:, None])[:, None, None, None, :]
    peak = jnp.maximum(jnp.max(jnp.where(live_mask, scores, -jnp.inf), axis=-1), self_score)
    weights = jnp.where(live_mask, jnp.exp(scores - peak[..., None]), 0.0)
    self_weight = jnp.exp(self_score - peak)
    totals = jnp.sum(weights, axis=-1) + self_weight
    lambda_grid = lam_heads.reshape(kv_heads, group_size)[None]
    combined = (
        weights[:, :, :, 0] / totals[:, :, :, 0, None]
        - lambda_grid[..., None] * weights[:, :, :, 1] / totals[:, :, :, 1, None]
    ).astype(jnp.bfloat16)
    self_combined = (
        self_weight[..., 0] / totals[..., 0] - lambda_grid * self_weight[..., 1] / totals[..., 1]
    ).astype(jnp.bfloat16)
    head_out = jnp.einsum(
        "skgc,sckv->skgv", combined, cache_values, preferred_element_type=jnp.float32
    )
    head_out = (
        head_out
        + self_combined.astype(jnp.float32)[..., None]
        * value_new.astype(jnp.float32)[:, :, None, :]
    )
    return rms_scale(head_out, head_gain, eps_head).astype(jnp.bfloat16).reshape(num_seqs, -1)


def expert_rows(row_block, routed_here, gate_one, up_one, down_one):
    slot_index = jnp.cumsum(routed_here) - 1
    pick_table = (
        (slot_index[None, :] == jnp.arange(EXP_CAP)[:, None]) & (routed_here[None, :] > 0)
    ).astype(jnp.bfloat16)
    picked = jnp.dot(pick_table, row_block, preferred_element_type=jnp.float32).astype(jnp.bfloat16)
    hidden = (
        jax.nn.silu(jnp.dot(picked, gate_one, preferred_element_type=jnp.float32))
        * jnp.dot(picked, up_one, preferred_element_type=jnp.float32)
    ).astype(jnp.bfloat16)
    result = jnp.dot(hidden, down_one, preferred_element_type=jnp.float32).astype(jnp.bfloat16)
    return jnp.dot(pick_table.T, result, preferred_element_type=jnp.float32)


def on_device(
    hidden_in,
    lengths,
    key_cache,
    value_cache,
    query_w,
    key_w,
    value_w,
    out_w,
    lam_heads,
    head_gain,
    attn_gain,
    moe_gain,
    routing,
    route_weight,
    gate_w,
    up_w,
    down_w,
    shared_gate,
    shared_up,
    shared_down,
):
    device = lax.axis_index("ep")
    tok_dev = hidden_in.shape[0]
    all_rows = lax.all_gather(hidden_in, "ep", axis=0, tiled=True)
    normed = rms_scale(all_rows, attn_gain, eps_norm).astype(jnp.bfloat16)
    joined_rows = jnp.concatenate([query_w, key_w, value_w], axis=1)
    column_block = lax.all_to_all(joined_rows, "ep", split_axis=1, concat_axis=0, tiled=True)
    column_sums = jnp.dot(normed, column_block, preferred_element_type=jnp.float32)
    projected = lax.all_to_all(column_sums, "ep", split_axis=0, concat_axis=1, tiled=True)
    query_cols = query_w.shape[1]
    key_cols = key_w.shape[1]
    queries = rotate(
        projected[:, :query_cols].reshape(tok_dev, KV_HEADS, -1, 2, HEAD_DIM),
        lengths[:, None, None, None],
    ).astype(jnp.bfloat16)
    key_new = rotate(
        projected[:, query_cols : query_cols + key_cols].reshape(tok_dev, KV_HEADS, 2, HEAD_DIM),
        lengths[:, None, None],
    ).astype(jnp.bfloat16)
    value_new = projected[:, query_cols + key_cols :].astype(jnp.bfloat16)
    attn_out = attend(
        queries, key_new, value_new, key_cache, value_cache, lengths, lam_heads, head_gain
    )
    pieces = lax.all_to_all(attn_out, "ep", split_axis=1, concat_axis=0, tiled=True)
    routed_here = jnp.sum((routing == device).astype(jnp.int32), axis=1)
    partial_value = jnp.dot(pieces, out_w, preferred_element_type=jnp.float32)
    attn_proj = lax.psum(partial_value, "ep").astype(jnp.bfloat16)
    mixer_all = (all_rows.astype(jnp.float32) + attn_proj.astype(jnp.float32)).astype(jnp.bfloat16)
    moe_all = rms_scale(mixer_all, moe_gain, eps_norm).astype(jnp.bfloat16)
    weight_col = jnp.sum(jnp.where(routing == device, route_weight, 0.0), axis=1)
    spread_back = (
        expert_rows(moe_all, routed_here, gate_w[0], up_w[0], down_w[0]) * weight_col[:, None]
    )
    routed = lax.psum_scatter(spread_back, "ep", scatter_dimension=0, tiled=True)
    after_mixer = lax.dynamic_slice_in_dim(mixer_all, device * tok_dev, tok_dev, 0)
    moe_in = lax.dynamic_slice_in_dim(moe_all, device * tok_dev, tok_dev, 0)
    shared_hidden = (
        jax.nn.silu(jnp.dot(moe_in, shared_gate, preferred_element_type=jnp.float32))
        * jnp.dot(moe_in, shared_up, preferred_element_type=jnp.float32)
    ).astype(jnp.bfloat16)
    shared_out = jnp.dot(shared_hidden, shared_down, preferred_element_type=jnp.float32)
    layer_out = (after_mixer.astype(jnp.float32) + routed + shared_out).astype(jnp.bfloat16)
    return (layer_out, key_new.reshape(tok_dev, -1), value_new)


def solution(mesh):
    placed = (
        P("ep", None),
        P("ep"),
        P("ep", None, None),
        P("ep", None, None),
        P("ep", None),
        P("ep", None),
        P("ep", None),
        P("ep", None),
        P(),
        P(),
        P(),
        P(),
        P(),
        P(),
        P("ep", None, None),
        P("ep", None, None),
        P("ep", None, None),
        P(),
        P(),
        P(),
    )
    return jax.shard_map(
        on_device,
        mesh=mesh,
        in_specs=placed,
        out_specs=(P("ep", None), P("ep", None), P("ep", None)),
        check_vma=False,
    )
```

profile of v0, /device:TPU:0, one launch (start us, length us, event | category | flops | bytes accessed | tf_op | source)
XLA Modules:
  0.0 275.9 jit_solution(12402558321039086071)
XLA Ops:
  7.2 1.2 pad_maximum_fusion
  8.4 0.5 all_to_all.40
  9.0 1.0 copy.52
  9.9 7.3 %all-to-all-start = ((bf16[64,32,96]{2,0,1:T(8,128)(2,1)}), bf16[64,32,96]{2,0,1:T(8,128)(2,1)S(1)}, u32[]{:S(2)}, u32[]{:S(2)}) async-start(bf16[64,32,96]{2,0,1:T(8,128)(2,1)} %copy.52), calls=%async_computation | async-start | bytes 1048576 | tf_op jit(solution)/shard_map/all_to_all | solution.py:119
  17.4 0.1 copy.63
  17.5 44.4 %all-gather = bf16[32,2,2048]{2,1,0:T(2,128)(2,1)S(1)} all-gather(bf16[1,2,2048]{2,1,0:T(2,128)(2,1)S(1)} %bitcast.88), channel_id=1, replica_groups=mesh['ep'=32] {'ep'}, dimensions={0}, use_global_device_ids=true | all-gather | bytes 270336 | tf_op jit(solution)/shard_map/all_gather | solution.py:116
  61.9 0.1 reshape.253
  62.0 0.1 multiply_reduce_fusion
  62.1 0.8 multiply_convert_fusion
  62.9 1.1 dot_general.41
  64.1 0.1 reduce-window.8
  64.2 0.1 multiply_cosine_fusion
  64.3 0.1 iota_compare_fusion.1
  64.4 0.2 fusion.32
  64.6 0.6 copy.55
  65.3 2.6 all-to-all-start.1
  67.8 0.1 add_reduce_fusion
  68.0 0.1 mul.256
  68.0 4.0 %reshape.245 = bf16[2,1024,2,2,128]{4,3,2,1,0:T(2,128)(2,1)} reshape(bf16[2,1024,512]{2,1,0:T(8,128)(2,1)} %param.22) | data formatting | bytes 4194304 | tf_op jit(solution)/shard_map/reshape | solution.py:42
  72.0 3.1 %all-to-all-done.1 = f32[32,2,96]{2,1,0:T(2,128)S(1)} async-done(((f32[32,2,96]{2,1,0:T(2,128)}), f32[32,2,96]{2,1,0:T(2,128)S(1)}, u32[]{:S(2)}, u32[]{:S(2)}) %all-to-all-start.1) | async-done | bytes 24608 | tf_op jit(solution)/shard_map/all_to_all | solution.py:121
  75.1 0.1 all_to_all.46
  75.3 0.1 fusion.67
  75.4 0.1 multiply_subtract_fusion
  75.5 0.1 fusion.79
  75.6 0.2 fusion.51
  75.8 2.5 select_reduce_fusion
  78.3 0.2 fusion.66
  78.6 0.5 multiply_reduce_fusion.1
  79.1 0.1 multiply_convert_fusion.1
  79.2 0.1 all_to_all.47
  79.3 0.6 copy.62
  79.9 2.7 all-to-all-start.2
  82.7 0.0 all-reduce.4.cloned.1.call-start
  82.7 0.1 maximum_convert_fusion
  82.8 0.6 convert_element_type.102
  83.4 6.5 %all-to-all-done.2 = bf16[2,32,64]{2,0,1:T(2,128)(2,1)S(1)} async-done(((bf16[2,32,64]{2,0,1:T(2,128)(2,1)}), bf16[2,32,64]{2,0,1:T(2,128)(2,1)S(1)}, u32[]{:S(2)}, u32[]{:S(2)}) %all-to-all-start.2) | async-done | bytes 8224 | tf_op jit(solution)/shard_map/all_to_all | solution.py:136
  89.8 0.2 fusion.68
  90.1 43.0 %all-reduce.5 = bf16[64,2048]{1,0:T(8,128)(2,1)S(1)} all-reduce(f32[64,2048]{1,0:T(8,128)S(1)} %fusion.68), channel_id=1, replica_groups=mesh['ep'=32] {'ep'}, use_global_device_ids=true, to_apply=%region_4.5 | all-reduce | flops 131072 | bytes 786432 | tf_op jit(solution)/shard_map/psum | solution.py:139
  133.0 0.2 fusion.29
  133.2 0.1 fusion.31
  133.4 0.2 convolution_convert_fusion.1
  133.5 2.1 fusion.7
  135.6 0.4 fusion.22
  136.0 1.4 convolution_multiply_fusion
  137.4 0.0 all-reduce.4.cloned.1.call-update
  137.4 2.0 fusion.55
  139.4 126.1 %all-reduce.4.cloned.1.call-done = f32[64,2048]{1,0:T(8,128)} async-done(((f32[64,2048]{1,0:T(8,128)}), f32[64,2048]{1,0:T(8,128)}) %all-reduce.4.cloned.1.call-update) | async-done | bytes 524304
  265.5 3.6 %fusion = bf16[2,2048]{1,0:T(2,128)(2,1)} fusion(bf16[512,2048]{1,0:T(8,128)(2,1)} %param.39, bf16[2048,512]{1,0:T(8,128)(2,1)} %param.38, f32[64,2048]{1,0:T(8,128)} %all-reduce.4.cloned.1.call-done, u32[]{:T(128)S(6)} %multiply.28, bf16[64,2048]{1,0:T(8,128)(2,1)S(1)} %get-tuple-element.6, s32[]{:T(128)S(6)} %select_n.17, f32[2,512]{1,0:T(2,128)S(1)} %fusion.55, ...), kind=kOutput, calls=%fused_computation.4 | convolution fusion | flops 8411136 | bytes 4240896 | tf_op jit(solution)/shard_map/dot_general | solution.py:153
  (46 shorter events, 0.3 us)
Async XLA Ops:
  7.2 128.9 %copy-start = (bf16[1,512,2048]{2,1,0:T(8,128)(2,1)S(1)}, bf16[1,512,2048]{2,1,0:T(8,128)(2,1)}, u32[]{:S(2)}) copy-start(bf16[1,512,2048]{2,1,0:T(8,128)(2,1)} %param.36) | copy-start | bytes 6291460
  7.2 10.1 %copy-start.10 = (s32[2]{0:T(128)S(1)}, s32[2]{0:T(128)}, u32[]{:S(2)}) copy-start(s32[2]{0:T(128)} %param.21) | copy-start | bytes 28
  7.2 10.1 %copy-start.7 = (f32[64,6]{0,1:T(8,128)S(1)}, f32[64,6]{0,1:T(8,128)}, u32[]{:S(2)}) copy-start(f32[64,6]{0,1:T(8,128)} %param.33) | copy-start | bytes 4612
  7.2 10.1 %copy-start.8 = (s32[64,6]{0,1:T(8,128)S(1)}, s32[64,6]{0,1:T(8,128)}, u32[]{:S(2)}) copy-start(s32[64,6]{0,1:T(8,128)} %param.32) | copy-start | bytes 4612
  7.2 10.3 %copy-start.5 = (bf16[2,2048]{1,0:T(2,128)(2,1)S(1)}, bf16[2,2048]{1,0:T(2,128)(2,1)}, u32[]{:S(2)}) copy-start(bf16[2,2048]{1,0:T(2,128)(2,1)} %param.20) | copy-start | bytes 24580
  8.9 53.2 %copy-start.3 = (f32[2048]{0:T(1024)S(1)}, f32[2048]{0:T(1024)}, u32[]{:S(2)}) copy-start(f32[2048]{0:T(1024)} %param.30) | copy-start | bytes 24580
  9.9 54.4 %all-to-all-start = ((bf16[64,32,96]{2,0,1:T(8,128)(2,1)}), bf16[64,32,96]{2,0,1:T(8,128)(2,1)S(1)}, u32[]{:S(2)}, u32[]{:S(2)}) async-start(bf16[64,32,96]{2,0,1:T(8,128)(2,1)} %copy.52), calls=%async_computation | async-start | bytes 1048576 | tf_op jit(solution)/shard_map/all_to_all | solution.py:119
  17.3 50.7 %copy-start.12 = (f32[8]{0:T(128)S(1)}, f32[8]{0:T(128)}, u32[]{:S(2)}) copy-start(f32[8]{0:T(128)} %param.28) | copy-start | bytes 100
  65.3 9.8 %all-to-all-start.1 = ((f32[32,2,96]{2,1,0:T(2,128)}), f32[32,2,96]{2,1,0:T(2,128)S(1)}, u32[]{:S(2)}, u32[]{:S(2)}) async-start(f32[32,2,96]{2,1,0:T(2,128)} %copy.55), calls=%async_computation.1 | async-start | bytes 65536 | tf_op jit(solution)/shard_map/all_to_all | solution.py:121
  75.2 3.9 %copy-start.6 = (bf16[2,512]{1,0:T(2,128)(2,1)}, bf16[2,512]{1,0:T(2,128)(2,1)S(1)}, u32[]{:S(2)}) copy-start(bf16[2,512]{1,0:T(2,128)(2,1)S(1)} %slice.101) | copy-start | bytes 6148
  75.3 3.3 %copy-start.11 = (bf16[2,1024,512]{2,1,0:T(8,128)(2,1)S(1)}, bf16[2,1024,512]{2,1,0:T(8,128)(2,1)}, u32[]{:S(2)}) copy-start(bf16[2,1024,512]{2,1,0:T(8,128)(2,1)} %param.23) | copy-start | bytes 6291460
  78.3 0.8 copy-start.9
  78.3 11.6 %copy-start.2 = (bf16[64,2048]{1,0:T(8,128)(2,1)S(1)}, bf16[64,2048]{1,0:T(8,128)(2,1)}, u32[]{:S(2)}) copy-start(bf16[64,2048]{1,0:T(8,128)(2,1)} %param.27) | copy-start | bytes 786436
  79.1 54.1 %copy-start.4 = (f32[2048]{0:T(1024)S(1)}, f32[2048]{0:T(1024)}, u32[]{:S(2)}) copy-start(f32[2048]{0:T(1024)} %param.31) | copy-start | bytes 24580
  79.9 9.9 %all-to-all-start.2 = ((bf16[2,32,64]{2,0,1:T(2,128)(2,1)}), bf16[2,32,64]{2,0,1:T(2,128)(2,1)S(1)}, u32[]{:S(2)}, u32[]{:S(2)}) async-start(bf16[2,32,64]{2,0,1:T(2,128)(2,1)} %copy.62), calls=%async_computation.2 | async-start | bytes 32768 | tf_op jit(solution)/shard_map/all_to_all | solution.py:136
  82.7 182.9 %all-reduce.4.cloned.1.call-start = ((), (), s32[]{:S(2)}) async-start(), calls=%async_computation.3 | async-start | bytes 1048576
  133.0 2.6 copy-start.1
Sparse Core Ops, SparseCore 0:
  137.5 127.9 all-reduce.3
where the time goes:
time: 276 us
  waiting for transfers between devices  136 us (49%)
  blocking collectives  87.4 us (32%)
  between operations  14.4 us (5%)
  matrix products  13.2 us (5%)
  starting transfers between devices  12.7 us (5%)
  local copies, waits for them, and re-layouts  9.12 us (3%)
  other arithmetic  3.5 us (1%)
    unnamed x2, waiting for transfers between devices  126 us
    all_gather x1, blocking collectives, on_device(): all_rows = lax.all_gather(hidden_in, 'ep', axis=0, tiled=True)  44.4 us
    psum x1, blocking collectives, on_device(): attn_proj = lax.psum(partial_value, 'ep').astype(jnp.bfloat16)  43 us
    all_to_all x1, starting transfers between devices, on_device(): lax.all_to_all(joined_rows, 'ep', split_axis=1, concat_axis=0, tiled=True)  7.33 us
    all_to_all x1, waiting for transfers between devices, on_device(): lax.all_to_all(attn_out, 'ep', split_axis=1, concat_axis=0, tiled=True)  6.46 us
  transfers between devices with their start and end apart: 4, of which 3 were waited for; matrix products, arithmetic and copies ran while one was open for 3% of the time, Pallas kernels for 0%

commit v1 on v0

--- a/solution.py
+++ b/solution.py
@@ -9,6 +9,12 @@
 eps_norm = 1e-06
 eps_head = 1e-05
 theta_base = 500000.0
+
+
+def add_all(value, mesh_axis):
+    blocks = lax.all_gather(value, mesh_axis, axis=0, tiled=False)
+    result = blocks.sum(axis=0)
+    return result
 
 
 def rms_scale(row_block, gain_vec, epsilon):
@@ -136,7 +142,7 @@
     pieces = lax.all_to_all(attn_out, "ep", split_axis=1, concat_axis=0, tiled=True)
     routed_here = jnp.sum((routing == device).astype(jnp.int32), axis=1)
     partial_value = jnp.dot(pieces, out_w, preferred_element_type=jnp.float32)
-    attn_proj = lax.psum(partial_value, "ep").astype(jnp.bfloat16)
+    attn_proj = add_all(partial_value, "ep").astype(jnp.bfloat16)
     mixer_all = (all_rows.astype(jnp.float32) + attn_proj.astype(jnp.float32)).astype(jnp.bfloat16)
     moe_all = rms_scale(mixer_all, moe_gain, eps_norm).astype(jnp.bfloat16)
     weight_col = jnp.sum(jnp.where(routing == device, route_weight, 0.0), axis=1)

time: 276 us -> 352 us (1.28)
  waiting for transfers between devices: 136 us -> 238 us
  blocking collectives: 87.4 us -> 54.4 us
  other arithmetic: 3.5 us -> 10.4 us
    all_gather x0 -> x1, waiting for transfers between devices: none -> 110 us  [add_all(): blocks = lax.all_gather(value, mesh_axis, axis=0, tiled=False)]
    psum x1 -> x0, blocking collectives: 43 us -> none  [on_device(): attn_proj = lax.psum(partial_value, 'ep').astype(jnp.bfloat16)]
    all_to_all x0 -> x1, blocking collectives: none -> 9.79 us  [on_device(): lax.all_to_all(attn_out, 'ep', split_axis=1, concat_axis=0, tiled=True)]
    reduce_sum x0 -> x1, other arithmetic: none -> 6.91 us  [add_all(): result = blocks.sum(axis=0)]
    all_to_all x1 -> x0, waiting for transfers between devices: 6.46 us -> none  [on_device(): lax.all_to_all(attn_out, 'ep', split_axis=1, concat_axis=0, tiled=True)]
    unnamed x2 -> x3, waiting for transfers between devices: 126 us -> 126 us
where the time goes in v1:
time: 352 us; the launch traced here: 351 us
  waiting for transfers between devices  238 us (68%)
  blocking collectives  54.4 us (15%)
  matrix products  15.5 us (4%)
  between operations  14.3 us (4%)
  other arithmetic  10.4 us (3%)
  starting transfers between devices  9.96 us (3%)
  local copies, waits for them, and re-layouts  8.52 us (2%)
    unnamed x3, waiting for transfers between devices  126 us
    all_gather x1, waiting for transfers between devices, add_all(): blocks = lax.all_gather(value, mesh_axis, axis=0, tiled=False)  110 us
    all_gather x1, blocking collectives, on_device(): all_rows = lax.all_gather(hidden_in, 'ep', axis=0, tiled=True)  44.6 us
    all_to_all x1, blocking collectives, on_device(): lax.all_to_all(attn_out, 'ep', split_axis=1, concat_axis=0, tiled=True)  9.79 us
    all_to_all x1, starting transfers between devices, on_device(): lax.all_to_all(joined_rows, 'ep', split_axis=1, concat_axis=0, tiled=True)  7.33 us
  transfers between devices with their start and end apart: 4, of which 3 were waited for; matrix products, arithmetic and copies ran while one was open for 3% of the time, Pallas kernels for 0%

profile of v1, /device:TPU:0, one launch (start us, length us, event | category | flops | bytes accessed | tf_op | source)
XLA Modules:
  0.0 351.4 jit_solution(2941904773761426140)
XLA Ops:
  7.2 1.2 pad_maximum_fusion
  8.4 0.5 all_to_all.40
  8.9 1.0 copy.52
  9.9 7.3 %all-to-all-start = ((bf16[64,32,96]{2,0,1:T(8,128)(2,1)}), bf16[64,32,96]{2,0,1:T(8,128)(2,1)S(1)}, u32[]{:S(2)}, u32[]{:S(2)}) async-start(bf16[64,32,96]{2,0,1:T(8,128)(2,1)} %copy.52), calls=%async_computation | async-start | bytes 1048576 | tf_op jit(solution)/shard_map/all_to_all | solution.py:125
  17.3 44.6 %all-gather.1 = bf16[32,2,2048]{2,1,0:T(2,128)(2,1)S(1)} all-gather(bf16[1,2,2048]{2,1,0:T(2,128)(2,1)S(1)} %bitcast.90), channel_id=1, replica_groups=mesh['ep'=32] {'ep'}, dimensions={0}, use_global_device_ids=true | all-gather | bytes 270336 | tf_op jit(solution)/shard_map/all_gather | solution.py:122
  61.9 0.1 reshape.254
  61.9 0.1 multiply_reduce_fusion
  62.1 0.8 multiply_convert_fusion
  62.9 1.1 dot_general.41
  64.1 0.1 iota_compare_fusion.1
  64.2 0.2 fusion.32
  64.4 0.6 copy.55
  65.1 2.6 all-to-all-start.1
  67.6 0.0 all-gather.4.cloned.1.call-start
  67.7 0.1 multiply_cosine_fusion
  67.8 4.0 %reshape.245 = bf16[2,1024,2,2,128]{4,3,2,1,0:T(2,128)(2,1)} reshape(bf16[2,1024,512]{2,1,0:T(8,128)(2,1)} %param.22) | data formatting | bytes 4194304 | tf_op jit(solution)/shard_map/reshape | solution.py:48
  71.8 0.1 mul.256
  71.8 3.0 all-to-all-done.1
  74.9 0.1 all_to_all.46
  75.1 0.1 fusion.67
  75.2 0.1 multiply_subtract_fusion
  75.2 0.1 fusion.79
  75.3 0.2 fusion.51
  75.5 2.4 select_reduce_fusion
  77.9 0.2 fusion.66
  78.2 2.1 multiply_reduce_fusion.1
  80.4 0.1 multiply_convert_fusion.1
  80.4 0.1 all_to_all.47
  80.5 9.8 %all_to_all.54 = bf16[2,32,64]{2,0,1:T(2,128)(2,1)S(1)} all-to-all(bf16[2,32,64]{2,0,1:T(2,128)(2,1)S(1)} %copy.62), channel_id=1, replica_groups=mesh['ep'=32] {'ep'}, dimensions={1} | all-to-all | bytes 16384 | tf_op jit(solution)/shard_map/all_to_all | solution.py:142
  90.3 1.0 fusion.68
  91.3 0.0 all-gather.4.cloned.1.call-update
  91.4 0.0 all-reduce.3.cloned.1.call-start
  91.5 0.1 copy.63
  91.6 0.1 reduce-window.8
  91.7 0.1 add_reduce_fusion
  91.8 0.1 maximum_convert_fusion
  91.9 0.6 convert_element_type.102
  92.5 109.8 %all-gather.4.cloned.1.call-done = f32[2048,2048]{1,0:T(8,128)} async-done(((f32[64,2048]{1,0:T(8,128)}), f32[2048,2048]{1,0:T(8,128)}) %all-gather.4.cloned.1.call-update) | async-done | bytes 16777232 | tf_op jit(solution)/shard_map/all_gather | solution.py:15
  202.2 6.9 %reduce_sum.66 = bf16[64,2048]{1,0:T(8,128)(2,1)S(1)} reduce(f32[32,64,2048]{2,1,0:T(8,128)} %bitcast.84, f32[]{:T(128)} %constant.15.clone.1), dimensions={0}, to_apply=%region_4.5 | reduce | flops 4063232 | bytes 17039364 | tf_op jit(solution)/shard_map/reduce_sum | solution.py:16
  209.2 0.2 fusion.29
  209.4 0.1 fusion.31
  209.5 0.2 convolution_convert_fusion.1
  209.7 2.1 fusion.7
  211.7 0.4 fusion.22
  212.2 1.4 convolution_multiply_fusion
  213.6 2.0 fusion.55
  215.5 125.5 %all-reduce.3.cloned.1.call-done = f32[64,2048]{1,0:T(8,128)} async-done(((f32[64,2048]{1,0:T(8,128)}), f32[64,2048]{1,0:T(8,128)}) %all-reduce.3.cloned.1.call-update) | async-done | bytes 524304
  341.0 3.6 %fusion = bf16[2,2048]{1,0:T(2,128)(2,1)} fusion(bf16[512,2048]{1,0:T(8,128)(2,1)} %param.39, bf16[2048,512]{1,0:T(8,128)(2,1)} %param.38, f32[64,2048]{1,0:T(8,128)} %all-reduce.3.cloned.1.call-done, u32[]{:T(128)S(6)} %multiply.28, bf16[64,2048]{1,0:T(8,128)(2,1)S(1)} %get-tuple-element.6, s32[]{:T(128)S(6)} %select_n.17, f32[2,512]{1,0:T(2,128)S(1)} %fusion.55, ...), kind=kOutput, calls=%fused_computation.4 | convolution fusion | flops 8411136 | bytes 4240896 | tf_op jit(solution)/shard_map/dot_general | solution.py:159
  (46 shorter events, 0.3 us)
Async XLA Ops:
  7.2 205.0 %copy-start = (bf16[1,512,2048]{2,1,0:T(8,128)(2,1)S(1)}, bf16[1,512,2048]{2,1,0:T(8,128)(2,1)}, u32[]{:S(2)}) copy-start(bf16[1,512,2048]{2,1,0:T(8,128)(2,1)} %param.36) | copy-start | bytes 6291460
  7.2 10.1 %copy-start.5 = (bf16[2,2048]{1,0:T(2,128)(2,1)S(1)}, bf16[2,2048]{1,0:T(2,128)(2,1)}, u32[]{:S(2)}) copy-start(bf16[2,2048]{1,0:T(2,128)(2,1)} %param.20) | copy-start | bytes 24580
  8.4 53.7 %copy-start.3 = (f32[2048]{0:T(1024)S(1)}, f32[2048]{0:T(1024)}, u32[]{:S(2)}) copy-start(f32[2048]{0:T(1024)} %param.30) | copy-start | bytes 24580
  9.9 54.1 %copy-start.10 = (s32[2]{0:T(128)S(1)}, s32[2]{0:T(128)}, u32[]{:S(2)}) copy-start(s32[2]{0:T(128)} %param.21) | copy-start | bytes 28
  9.9 54.2 %all-to-all-start = ((bf16[64,32,96]{2,0,1:T(8,128)(2,1)}), bf16[64,32,96]{2,0,1:T(8,128)(2,1)S(1)}, u32[]{:S(2)}, u32[]{:S(2)}) async-start(bf16[64,32,96]{2,0,1:T(8,128)(2,1)} %copy.52), calls=%async_computation | async-start | bytes 1048576 | tf_op jit(solution)/shard_map/all_to_all | solution.py:125
  65.1 9.8 %all-to-all-start.1 = ((f32[32,2,96]{2,1,0:T(2,128)}), f32[32,2,96]{2,1,0:T(2,128)S(1)}, u32[]{:S(2)}, u32[]{:S(2)}) async-start(f32[32,2,96]{2,1,0:T(2,128)} %copy.55), calls=%async_computation.1 | async-start | bytes 65536 | tf_op jit(solution)/shard_map/all_to_all | solution.py:127
  67.6 134.6 %all-gather.4.cloned.1.call-start = ((), (), s32[]{:S(2)}) async-start(), calls=%async_computation.3 | async-start | bytes 17301504 | tf_op jit(solution)/shard_map/all_gather | solution.py:15
  67.8 4.0 %copy-start.11 = (f32[8]{0:T(128)S(1)}, f32[8]{0:T(128)}, u32[]{:S(2)}) copy-start(f32[8]{0:T(128)} %param.28) | copy-start | bytes 100
  75.0 5.3 %copy-start.6 = (bf16[2,512]{1,0:T(2,128)(2,1)}, bf16[2,512]{1,0:T(2,128)(2,1)S(1)}, u32[]{:S(2)}) copy-start(bf16[2,512]{1,0:T(2,128)(2,1)S(1)} %slice.101) | copy-start | bytes 6148
  77.9 2.4 copy-start.9
  77.9 12.4 %copy-start.2 = (bf16[64,2048]{1,0:T(8,128)(2,1)S(1)}, bf16[64,2048]{1,0:T(8,128)(2,1)}, u32[]{:S(2)}) copy-start(bf16[64,2048]{1,0:T(8,128)(2,1)} %param.27) | copy-start | bytes 786436
  78.2 13.2 %copy-start.7 = (f32[64,6]{0,1:T(8,128)S(1)}, f32[64,6]{0,1:T(8,128)}, u32[]{:S(2)}) copy-start(f32[64,6]{0,1:T(8,128)} %param.33) | copy-start | bytes 4612
  78.2 13.2 %copy-start.8 = (s32[64,6]{0,1:T(8,128)S(1)}, s32[64,6]{0,1:T(8,128)}, u32[]{:S(2)}) copy-start(s32[64,6]{0,1:T(8,128)} %param.32) | copy-start | bytes 4612
  91.4 249.7 %all-reduce.3.cloned.1.call-start = ((), (), s32[]{:S(2)}) async-start(), calls=%async_computation.4 | async-start | bytes 1048576
  202.2 7.1 %copy-start.4 = (f32[2048]{0:T(1024)S(1)}, f32[2048]{0:T(1024)}, u32[]{:S(2)}) copy-start(f32[2048]{0:T(1024)} %param.31) | copy-start | bytes 24580
  209.1 2.6 copy-start.1
Sparse Core Ops, SparseCore 0:
  91.5 110.6 all-gather.3
  213.7 127.3 all-reduce.2
